TPU v7x, 512 devices: a whole 4x4x16 slice. The times are simulated.
512 devices in a mesh: sp: 16 (over z), fs: 4 (over y), tp: 8 (over x, core).
Axes of the slice: x: 4, y: 4, z: 16, core: 2. Of those that a mesh axis runs over, the one named last changes fastest.
Arguments:
- tokens: bfloat16 [4, 16384, 2048], P('fs', 'sp', 'tp'), may hold values from -8 to 8
- norm_gain: float32 [2048], replicated, may hold values from 0.1 to 1.9
- w_query: bfloat16 [2048, 1024], P(('sp', 'fs'), 'tp'), may hold values from -4 to 4
- w_key: bfloat16 [2048, 512], P(('sp', 'fs'), 'tp'), may hold values from -0.16 to 0.16
- w_value: bfloat16 [2048, 512], P(('sp', 'fs'), 'tp'), may hold values from -0.125 to 0.125
- w_conv_in: bfloat16 [2048, 1024], P(('sp', 'fs'), 'tp'), may hold values from -0.125 to 0.125
- w_conv_b: bfloat16 [2048, 1024], P(('sp', 'fs'), 'tp'), may hold values from -0.125 to 0.125
- w_conv_c: bfloat16 [2048, 1024], P(('sp', 'fs'), 'tp'), may hold values from -0.125 to 0.125
- conv_taps: bfloat16 [3, 1024], P(None, 'tp'), may hold values from -3.5 to 3.5
- sink_logits: float32 [16], P('tp'), may hold values from 1 to 5
- w_attn_out: bfloat16 [1024, 2048], P('tp', ('sp', 'fs')), may hold values from -0.375 to 0.375
- w_conv_out: bfloat16 [1024, 2048], P('tp', ('sp', 'fs')), may hold values from -0.125 to 0.125
Outputs:
- mixed: bfloat16 [4, 16384, 2048], P('fs', ('sp', 'tp'))
All inputs are finite; a program needn't handle non-finite values.
Results may differ from a plain program's by a relative error of at most 0.02.
Values may be sent and summed in bfloat16 or wider, within the bound.
A program may use at most 128 MiB of HBM per device.

v0:
```python
import jax
import jax.numpy as jnp
from jax import lax
from jax.sharding import PartitionSpec as P

HEADS = 16
HEAD = 64
WINDOW = 128


def in_one_piece(arrays, axis, dim, along):
    widths = [a.shape[along] for a in arrays]
    both = jnp.concatenate(arrays, axis=along)
    whole = lax.all_gather(both, axis, axis=dim, tiled=True)
    return tuple(jnp.split(whole, [sum(widths[:k]) for k in range(1, len(widths))], axis=along))


def shifted(block, axis, distance):
    devices = range(lax.axis_size(axis))
    route = [(i - distance, i) for i in devices if i - distance in devices]
    return lax.ppermute(block, axis, route)


def rows_first(arrays, axis, dims):
    turned = [jnp.moveaxis(a, dim, 0) for a, dim in zip(arrays, dims)]
    both = jnp.concatenate([t.reshape(len(t), -1) for t in turned], axis=1)
    whole, at, finished = (lax.all_gather(both, axis, axis=0, tiled=True), 0, [])
    for t, dim in zip(turned, dims):
        share = whole[:, at : at + t[0].size].reshape(-1, *t.shape[1:])
        finished.append(jnp.moveaxis(share, 0, dim))
        at += t[0].size
    return tuple(finished)


def norm_rows(tokens, norm_gain):
    values = tokens.astype(jnp.float32)
    average = jnp.mean(values, axis=-1, keepdims=True)
    centred = values - average
    variance = jnp.mean(centred * centred, axis=-1, keepdims=True)
    return (centred * lax.rsqrt(variance + 1e-05) * norm_gain).astype(jnp.bfloat16)


def attend(queries, keys_values, earlier_rows, sink_logits, head_base, row_base):
    row_total = queries.shape[0]
    kv_cols = keys_values.shape[1] // 2
    kv_here = kv_cols // HEAD
    heads_here = queries.shape[1] // HEAD
    group = heads_here // kv_here
    keys_all = jnp.concatenate([earlier_rows, keys_values], axis=0)
    block_rows = min(512, row_total)
    head_ids = head_base + jnp.arange(heads_here, dtype=jnp.int32)
    slopes = jnp.exp2(-8.0 * (head_ids + 1).astype(jnp.float32) / HEADS).reshape(kv_here, group)[
        :, :, None, None
    ]
    sinks = sink_logits.reshape(kv_here, group)[:, :, None, None]
    row_ids = jnp.arange(block_rows, dtype=jnp.int32)[:, None]
    col_ids = jnp.arange(block_rows + WINDOW, dtype=jnp.int32)[None, :]
    distance = WINDOW + row_ids - col_ids
    outputs = []
    for block in range(row_total // block_rows):
        first_row = block * block_rows
        query_block = queries[first_row : first_row + block_rows].reshape(
            block_rows, kv_here, group, HEAD
        )
        band = keys_all[first_row : first_row + block_rows + WINDOW]
        band_keys = band[:, :kv_cols].reshape(block_rows + WINDOW, kv_here, HEAD)
        band_values = band[:, kv_cols:].reshape(block_rows + WINDOW, kv_here, HEAD)
        scores = jnp.einsum(
            "qkgd,skd->kgqs", query_block, band_keys, preferred_element_type=jnp.float32
        ) * HEAD ** (-0.5)
        scores = scores - slopes * distance.astype(jnp.float32)
        key_place = row_base + first_row - WINDOW + col_ids
        keep = (distance >= 0) & (distance < WINDOW) & (key_place >= 0)
        scores = jnp.where(keep, scores, -jnp.inf)
        highest = jnp.maximum(jnp.max(scores, axis=-1, keepdims=True), sinks)
        raised = jnp.exp(scores - highest)
        denominator = jnp.sum(raised, axis=-1, keepdims=True) + jnp.exp(sinks - highest)
        weights = (raised / denominator).astype(jnp.bfloat16)
        mixed = jnp.einsum(
            "kgqs,skd->qkgd", weights, band_values, preferred_element_type=jnp.float32
        )
        outputs.append(mixed.astype(jnp.bfloat16).reshape(block_rows, heads_here * HEAD))
    return jnp.concatenate(outputs, axis=0)


def on_device(
    tokens,
    norm_gain,
    w_query,
    w_key,
    w_value,
    w_conv_in,
    w_conv_b,
    w_conv_c,
    conv_taps,
    sink_logits,
    w_attn_out,
    w_conv_out,
):
    gathered = lax.all_gather(tokens, "tp", axis=2, tiled=True)[0]
    normed = norm_rows(gathered, norm_gain)
    row_total = normed.shape[0]
    weight_rows = in_one_piece(
        (w_query, w_key, w_value, w_conv_in, w_conv_b, w_conv_c), ("sp", "fs"), 0, 1
    )
    results = tuple(
        (
            jnp.dot(normed, rows_part, preferred_element_type=jnp.float32)
            for rows_part in weight_rows
        )
    )
    queries, keys, values, inner, gate_b, gate_c = tuple(
        (result.astype(jnp.bfloat16) for result in results)
    )
    product = (gate_c.astype(jnp.float32) * inner.astype(jnp.float32)).astype(jnp.bfloat16)
    keys_values = jnp.concatenate([keys, values], axis=1)
    earlier_kv, earlier_product = shifted(
        (keys_values[row_total - WINDOW :], product[row_total - 2 :]), "sp", 1
    )
    heads_here = queries.shape[1] // HEAD
    head_base = lax.axis_index("tp") * heads_here
    row_base = lax.axis_index("sp") * row_total
    attended = attend(queries, keys_values, earlier_kv, sink_logits, head_base, row_base)
    taps = conv_taps.astype(jnp.float32)
    padded = jnp.concatenate([earlier_product, product], axis=0).astype(jnp.float32)
    filtered = (
        taps[0] * padded[0:row_total]
        + taps[1] * padded[1 : row_total + 1]
        + taps[2] * padded[2 : row_total + 2]
    )
    conv_out = (gate_b.astype(jnp.float32) * filtered).astype(jnp.bfloat16)
    attn_columns, conv_columns = rows_first((w_attn_out, w_conv_out), ("sp", "fs"), (1, 1))
    summed = lax.psum_scatter(
        (
            jnp.dot(attended, attn_columns, preferred_element_type=jnp.float32)
            + jnp.dot(conv_out, conv_columns, preferred_element_type=jnp.float32)
        ).astype(jnp.bfloat16),
        "tp",
        scatter_dimension=0,
        tiled=True,
    )
    return summed[None]


def solution(mesh):
    placed = (
        P("fs", "sp", "tp"),
        P(),
        P(("sp", "fs"), "tp"),
        P(("sp", "fs"), "tp"),
        P(("sp", "fs"), "tp"),
        P(("sp", "fs"), "tp"),
        P(("sp", "fs"), "tp"),
        P(("sp", "fs"), "tp"),
        P(None, "tp"),
        P("tp"),
        P("tp", ("sp", "fs")),
        P("tp", ("sp", "fs")),
    )
    return jax.shard_map(
        on_device,
        mesh=mesh,
        in_specs=placed,
        out_specs=P("fs", ("sp", "tp"), None),
        check_vma=False,
    )
```

profile of v0, /device:TPU:8, one launch (start us, length us, event | category | flops | bytes accessed | tf_op | source)
XLA Modules:
  0.0 406.5 jit_solution(2349871307167087293)
XLA Ops:
  6.5 0.7 all-gather.4.cloned.1.call-update
  7.3 1.5 concatenate.18
  8.9 1.3 pad_maximum_fusion.4
  10.3 0.7 convert_element_type.108
  11.0 1.2 fusion.14
  12.2 0.5 fusion.32
  12.7 44.3 %all-gather.4.cloned.1.call-done = bf16[1,1024,2048]{2,1,0:T(8,128)(2,1)} async-done(((bf16[1,1024,256]{2,1,0:T(8,128)(2,1)}), bf16[1,1024,2048]{2,1,0:T(8,128)(2,1)}) %all-gather.4.cloned.1.call-update) | async-done | bytes 4194320 | tf_op jit(solution)/shard_map/all_gather | solution.py:100
  57.0 3.0 convert_reduce_fusion
  60.0 0.5 copy-done.1
  60.5 1.2 fusion.3
  61.7 3.0 fusion.5
  64.7 137.2 %all-gather.6.cloned.1.call-done = bf16[2048,640]{1,0:T(8,128)(2,1)} async-done(((bf16[32,640]{1,0:T(8,128)(2,1)}), bf16[2048,640]{1,0:T(8,128)(2,1)}) %all-gather.6.cloned.1.call-update) | async-done | bytes 2621456 | tf_op jit(solution)/shard_map/all_gather | solution.py:14
  201.9 3.9 convolution_convert_fusion.4
  205.8 2.6 convolution_convert_fusion.5
  208.4 3.7 collective-permute-start
  212.1 1.5 convolution_convert_fusion.3
  213.7 1.2 fusion.21
  214.9 1.3 fusion.20
  216.2 2.4 collective-permute-start.1
  218.7 0.9 fusion.65
  219.5 0.2 collective-permute-done.1
  219.8 0.9 fusion.64
  220.8 0.4 fusion.8
  221.1 0.1 exponential_add_fusion.1
  221.2 0.4 fusion.9
  221.6 0.1 exponential_add_fusion
  221.7 0.6 fusion.28
  222.3 0.6 fusion.25
  222.8 117.6 %all-gather.8.cloned.1.call-done = bf16[2048,256]{1,0:T(8,128)(2,1)} async-done(((bf16[32,256]{1,0:T(8,128)(2,1)}), bf16[2048,256]{1,0:T(8,128)(2,1)}) %all-gather.8.cloned.1.call-update) | async-done | bytes 1048592 | tf_op jit(solution)/shard_map/all_gather | solution.py:27
  340.4 5.6 %fusion.42 = f32[1024,2048]{1,0:T(8,128)} fusion(bf16[2048,256]{1,0:T(8,128)(2,1)} %all-gather.8.cloned.1.call-done, bf16[512,128]{0,1:T(8,128)(2,1)S(1)} %bitcast.77, bf16[512,128]{0,1:T(8,128)(2,1)S(1)} %bitcast.78), kind=kOutput, calls=%fused_computation.54 | convolution fusion | flops 537395200 | bytes 9175040 | tf_op jit(solution)/shard_map/dot_general | solution.py:135
  345.9 11.1 %add_convert_fusion = bf16[1024,2048]{1,0:T(8,128)(2,1)} fusion(f32[1024,2048]{1,0:T(8,128)} %fusion.42, bf16[1024,2048]{1,0:T(8,128)(2,1)} %fusion.5, bf16[2048,256]{1,0:T(8,128)(2,1)} %all-gather.8.cloned.1.call-done, f32[1026,128]{1,0:T(8,128)S(1)} %maximum_convert_fusion, bf16[2048,640]{1,0:T(8,128)(2,1)S(1)} %copy-done.2, f32[128]{0:T(128)S(1)} %get-tuple-element.8, ...), kind=kOutput, calls=%fused_computation.8 | convolution fusion | flops 1079115776 | bytes 19400192 | tf_op jit(solution)/shard_map/dot_general | solution.py:136
  357.1 42.9 %reduce-scatter.2.cloned.1.call-done = bf16[128,2048]{1,0:T(8,128)(2,1)} async-done(((bf16[1024,2048]{1,0:T(8,128)(2,1)}), bf16[128,2048]{1,0:T(8,128)(2,1)}) %reduce-scatter.2.cloned.1.call-update) | async-done | bytes 524304 | tf_op jit(solution)/shard_map/reduce_scatter | solution.py:133
  (30 shorter events, 0.4 us)
Async XLA Ops:
  6.5 50.5 %all-gather.4.cloned.1.call-start = ((), (), s32[]{:S(2)}) async-start(), calls=%async_computation.1 | async-start | bytes 4718592 | tf_op jit(solution)/shard_map/all_gather | solution.py:100
  7.3 194.6 %all-gather.6.cloned.1.call-start = ((), (), s32[]{:S(2)}) async-start(), calls=%async_computation.2 | async-start | bytes 2662400 | tf_op jit(solution)/shard_map/all_gather | solution.py:14
  8.8 331.6 %all-gather.8.cloned.1.call-start = ((), (), s32[]{:S(2)}) async-start(), calls=%async_computation.3 | async-start | bytes 1064960 | tf_op jit(solution)/shard_map/all_gather | solution.py:27
  10.2 389.8 %reduce-scatter.2.cloned.1.call-start = ((), (), s32[]{:S(2)}) async-start(), calls=%async_computation.4 | async-start | bytes 4718592 | tf_op jit(solution)/shard_map/reduce_scatter | solution.py:133
  57.0 3.4 copy-start.1
  60.0 1.7 copy-start.4
  201.9 3.9 copy-start
  205.8 6.3 %copy-start.2 = (bf16[2048,640]{1,0:T(8,128)(2,1)S(1)}, bf16[2048,640]{1,0:T(8,128)(2,1)}, u32[]{:S(2)}) copy-start(bf16[2048,640]{1,0:T(8,128)(2,1)} %all-gather.6.cloned.1.call-done) | copy-start | bytes 7864324
  208.4 11.4 %collective-permute-start = (bf16[128,128]{0,1:T(8,128)(2,1)S(1)}, bf16[128,128]{0,1:T(8,128)(2,1)S(1)}, u32[]{:S(2)}, u32[]{:S(2)}) collective-permute-start(bf16[128,128]{0,1:T(8,128)(2,1)S(1)} %pad_maximum_fusion.3), channel_id=1, source_target_pairs={{0,32},{32,64},{64,96},{96,128},{128,160},{160,192},{192,224},{224... | collective-permute-start | bytes 98312 | tf_op jit(solution)/shard_map/ppermute | solution.py:21
  214.9 3.7 copy-start.3
  216.2 3.5 collective-permute-start.1
  219.5 1.2 copy-start.5
Sparse Core Ops, SparseCore 0:
  9.4 47.5 all-gather.3
  60.0 141.8 all-gather.5
  204.8 135.5 all-gather.7
  357.2 42.6 reduce-scatter.1
where the time goes:
time: 407 us; the launch traced here: 406 us
  waiting for transfers between devices  343 us (84%)
  matrix products  30.1 us (7%)
  between operations  13.3 us (3%)
  other arithmetic  12 us (3%)
  starting transfers between devices  6.25 us (2%)
    all_gather x1, waiting for transfers between devices, in_one_piece(): whole = lax.all_gather(both, axis, axis=dim, tiled=True)  137 us
    all_gather x1, waiting for transfers between devices, rows_first(): lax.all_gather(both, axis, axis=0, tiled=True)  118 us
    all_gather x1, waiting for transfers between devices, on_device(): gathered = lax.all_gather(tokens, 'tp', axis=2, tiled=True)[0]  44.3 us
    reduce_scatter x1, waiting for transfers between devices, on_device(): lax.psum_scatter((jnp.dot(attended, attn_columns, preferred_element_type=...  42.9 us
    dot_general x1, matrix products, on_device(): jnp.dot(conv_out, conv_columns, preferred_element_type=jnp.float32)  11.1 us
    dot_general x5, matrix products, on_device(): jnp.dot(normed, rows_part, preferred_element_type=jnp.float32)  10.5 us
  transfers between devices with their start and end apart: 6, of which 5 were waited for; matrix products, arithmetic and copies ran while one was open for 7% of the time, Pallas kernels for 0%

commit v1 on v0

--- a/solution.py
+++ b/solution.py
@@ -6,6 +6,14 @@
 HEADS = 16
 HEAD = 64
 WINDOW = 128
+
+
+def gather_from_all(value, axis, dim):
+    size = lax.axis_size(axis)
+    repeats = [size if d == dim else 1 for d in range(value.ndim)]
+    return lax.all_to_all(
+        jnp.tile(value, repeats), axis, split_axis=dim, concat_axis=dim, tiled=True
+    )
 
 
 def in_one_piece(arrays, axis, dim, along):
@@ -97,7 +105,7 @@
     w_attn_out,
     w_conv_out,
 ):
-    gathered = lax.all_gather(tokens, "tp", axis=2, tiled=True)[0]
+    gathered = gather_from_all(tokens, "tp", 2)[0]
     normed = norm_rows(gathered, norm_gain)
     row_total = normed.shape[0]
     weight_rows = in_one_piece(

time: 407 us -> 361 us (0.89)
  waiting for transfers between devices: 343 us -> 196 us
  other arithmetic: 12 us -> 59.8 us
  local copies, waits for them, and re-layouts: 2.01 us -> 49.2 us
  starting transfers between devices: 6.25 us -> 12.6 us
    all_gather x1, waiting for transfers between devices: 137 us -> 0.01 us  [in_one_piece(): whole = lax.all_gather(both, axis, axis=dim, tiled=True)]
    all_to_all x0 -> x1, waiting for transfers between devices: none -> 48.1 us  [gather_from_all(): lax.all_to_all(jnp.tile(value, repeats), axis, split_axis=dim, concat_axi...]
    all_gather x1 -> x0, waiting for transfers between devices: 44.3 us -> none  [on_device(): gathered = lax.all_gather(tokens, 'tp', axis=2, tiled=True)[0]]
    another operation x0 -> x3, local copies, waits for them, and re-layouts: none -> 30.5 us  [gather_from_all(): jnp.tile(value, repeats)]
    unnamed x0 -> x1, other arithmetic: none -> 25.9 us
    unnamed x12 -> x21, local copies, waits for them, and re-layouts: 0.5 us -> 17.2 us
    reduce_sum x1, other arithmetic: 2.95 us -> 17.5 us  [norm_rows(): average = jnp.mean(values, axis=-1, keepdims=True)]
    all_gather x1, waiting for transfers between devices: 118 us -> 105 us  [rows_first(): lax.all_gather(both, axis, axis=0, tiled=True)]
  transfers between devices with their start and end apart: 6 -> 6, of which waited for: 5 -> 4; matrix products, arithmetic and copies ran while one was open for 7% -> 33% of each run, Pallas kernels for 0% -> 0%
where the time goes in v1:
time: 361 us; the launch traced here: 360 us
  waiting for transfers between devices  196 us (54%)
  other arithmetic  59.8 us (17%)
  local copies, waits for them, and re-layouts  49.2 us (14%)
  matrix products  28.7 us (8%)
  between operations  13.4 us (4%)
  starting transfers between devices  12.6 us (3%)
    all_gather x1, waiting for transfers between devices, rows_first(): lax.all_gather(both, axis, axis=0, tiled=True)  105 us
    all_to_all x1, waiting for transfers between devices, gather_from_all(): lax.all_to_all(jnp.tile(value, repeats), axis, split_axis=dim, concat_axi...  48.1 us
    reduce_scatter x1, waiting for transfers between devices, on_device(): lax.psum_scatter((jnp.dot(attended, attn_columns, preferred_element_type=...  42.9 us
    another operation x3, local copies, waits for them, and re-layouts, gather_from_all(): jnp.tile(value, repeats)  30.5 us
    unnamed x1, other arithmetic  25.9 us
    reduce_sum x1, other arithmetic, norm_rows(): average = jnp.mean(values, axis=-1, keepdims=True)  17.5 us
    unnamed x21, local copies, waits for them, and re-layouts  17.2 us
    dot_general x1, matrix products, on_device(): jnp.dot(conv_out, conv_columns, preferred_element_type=jnp.float32)  11.2 us
  transfers between devices with their start and end apart: 6, of which 4 were waited for; matrix products, arithmetic and copies ran while one was open for 33% of the time, Pallas kernels for 0%

profile of v1, /device:TPU:8, one launch (start us, length us, event | category | flops | bytes accessed | tf_op | source)
XLA Modules:
  0.0 360.1 jit_solution(1863694634059414918)
XLA Ops:
  6.5 1.5 concatenate.18
  8.0 1.2 copy.18
  9.3 0.5 tile.12
  9.8 28.7 %copy.31 = bf16[1,1024,2048]{1,0,2:T(2,128)(2,1)} copy(bf16[1,1024,2048]{1,2,0:T(8,128)(2,1)S(1)} %bitcast.78) | data formatting | bytes 8388608 | tf_op jit(solution)/shard_map/tile | solution.py:15
  38.6 0.5 broadcast.214
  39.1 25.9 %reduce.5 = bf16[2048,1024]{1,0:T(8,128)(2,1)} reduce(bf16[2048,1,1024]{2,1,0:T(2,128)(2,1)} %bitcast.77, bf16[]{:T(256)} %broadcast.214), dimensions={1}, to_apply=%bitcast.76.reduce_sub_computation | reduce | bytes 8388610
  64.9 7.8 %reshape.255 = bf16[8,2,131072]{2,1,0:T(2,128)(2,1)} reshape(bf16[2048,1024]{1,0:T(8,128)(2,1)} %reduce.5) | data formatting | bytes 8388608
  72.7 4.7 %all-to-all-start = ((bf16[8,2,131072]{2,1,0:T(2,128)(2,1)}), bf16[8,2,131072]{2,1,0:T(2,128)(2,1)}, u32[]{:S(2)}, u32[]{:S(2)}) async-start(bf16[8,2,131072]{2,1,0:T(2,128)(2,1)} %reshape.255), calls=%async_computation | async-start | bytes 8388608 | tf_op jit(solution)/shard_map/all_to_all | solution.py:14
  77.5 0.6 pad_maximum_fusion.4
  78.3 0.5 fusion.26
  79.0 48.1 %all-to-all-done = bf16[8,2,131072]{2,1,0:T(2,128)(2,1)} async-done(((bf16[8,2,131072]{2,1,0:T(2,128)(2,1)}), bf16[8,2,131072]{2,1,0:T(2,128)(2,1)}, u32[]{:S(2)}, u32[]{:S(2)}) %all-to-all-start) | async-done | bytes 4194336 | tf_op jit(solution)/shard_map/all_to_all | solution.py:14
  127.1 8.8 %reshape.256 = bf16[2048,1,1024]{2,1,0:T(2,128)(2,1)} reshape(bf16[8,2,131072]{2,1,0:T(2,128)(2,1)} %all-to-all-done) | data formatting | bytes 8388608
  135.9 10.1 %bitcast_convert_fusion = f32[1,1024,2048]{1,0,2:T(1,128)S(1)} fusion(bf16[2048,1,1024]{2,1,0:T(2,128)(2,1)} %reshape.256), kind=kLoop, calls=%fused_computation.94 | loop fusion | flops 2097152 | bytes 12582912 | tf_op jit(solution)/shard_map/convert_element_type | solution.py:44
  146.0 17.5 %convert_reduce_fusion = f32[1024]{0:T(1024)S(1)} fusion(bf16[2048,1,1024]{2,1,0:T(2,128)(2,1)S(1)} %copy-done.1), kind=kLoop, calls=%fused_computation.90 | loop fusion | flops 4193280 | bytes 4198400 | tf_op jit(solution)/shard_map/reduce_sum | solution.py:45
  163.6 1.2 multiply_reduce_fusion
  164.8 2.7 multiply_convert_fusion
  167.6 3.5 convolution_convert_fusion.4
  171.2 2.1 convolution_convert_fusion.5
  173.3 4.0 %collective-permute-start = (bf16[128,128]{0,1:T(8,128)(2,1)S(1)}, bf16[128,128]{0,1:T(8,128)(2,1)S(1)}, u32[]{:S(2)}, u32[]{:S(2)}) collective-permute-start(bf16[128,128]{0,1:T(8,128)(2,1)S(1)} %pad_maximum_fusion.3), channel_id=1, source_target_pairs={{0,32},{32,64},{64,96},{96,128},{128,160},{160,192},{192,224},{224... | collective-permute-start | bytes 98312 | tf_op jit(solution)/shard_map/ppermute | solution.py:29
  177.3 0.8 convolution_convert_fusion.3
  178.1 1.3 fusion.15
  179.4 1.3 fusion.14
  180.7 3.8 %collective-permute-start.1 = (bf16[2,128]{1,0:T(2,128)(2,1)S(1)}, bf16[2,128]{1,0:T(2,128)(2,1)S(1)}, u32[]{:S(2)}, u32[]{:S(2)}) collective-permute-start(bf16[2,128]{1,0:T(2,128)(2,1)S(1)} %slice.77), channel_id=1, source_target_pairs={{0,32},{32,64},{64,96},{96,128},{128,160},{160,192},{192,224},{224... | collective-permute-start | bytes 1544 | tf_op jit(solution)/shard_map/ppermute | solution.py:29
  184.6 0.9 fusion.59
  185.5 0.4 collective-permute-done.1
  185.9 0.9 fusion.58
  187.8 0.6 fusion.22
  188.4 0.6 fusion.19
  189.0 104.9 %all-gather.5.cloned.1.call-done = bf16[2048,256]{1,0:T(8,128)(2,1)} async-done(((bf16[32,256]{1,0:T(8,128)(2,1)}), bf16[2048,256]{1,0:T(8,128)(2,1)}) %all-gather.5.cloned.1.call-update) | async-done | bytes 1048592 | tf_op jit(solution)/shard_map/all_gather | solution.py:35
  293.9 5.7 %fusion.36 = f32[1024,2048]{1,0:T(8,128)} fusion(bf16[2048,256]{1,0:T(8,128)(2,1)} %all-gather.5.cloned.1.call-done, bf16[512,128]{0,1:T(8,128)(2,1)S(1)} %bitcast.80, bf16[512,128]{0,1:T(8,128)(2,1)S(1)} %bitcast.81), kind=kOutput, calls=%fused_computation.49 | convolution fusion | flops 537395200 | bytes 9175040 | tf_op jit(solution)/shard_map/dot_general | solution.py:143
  299.6 11.2 %add_convert_fusion = bf16[1024,2048]{1,0:T(8,128)(2,1)} fusion(f32[1024,2048]{1,0:T(8,128)} %fusion.36, bf16[1024,2048]{0,1:T(8,128)(2,1)} %multiply_convert_fusion, bf16[2048,256]{1,0:T(8,128)(2,1)S(1)} %copy-done.2, f32[1026,128]{1,0:T(8,128)S(1)} %maximum_convert_fusion, bf16[2048,640]{1,0:T(8,128)(2,1)} %all-gather.3.cloned.1.call-done, ...), kind=kOutput, calls=%fused_computation.1 | convolution fusion | flops 1079115776 | bytes 19400192 | tf_op jit(solution)/shard_map/dot_general | solution.py:144
  310.7 42.9 %reduce-scatter.2.cloned.1.call-done = bf16[128,2048]{1,0:T(8,128)(2,1)} async-done(((bf16[1024,2048]{1,0:T(8,128)(2,1)}), bf16[128,2048]{1,0:T(8,128)(2,1)}) %reduce-scatter.2.cloned.1.call-update) | async-done | bytes 524304 | tf_op jit(solution)/shard_map/reduce_scatter | solution.py:141
  (43 shorter events, 1.6 us)
Async XLA Ops:
  6.5 161.0 %all-gather.3.cloned.1.call-start = ((), (), s32[]{:S(2)}) async-start(), calls=%async_computation.2 | async-start | bytes 2662400 | tf_op jit(solution)/shard_map/all_gather | solution.py:22
  72.7 4.8 %copy-start.5 = (bf16[128,32]{0,1:T(8,128)(2,1)S(1)}, bf16[128,32]{0,1:T(8,128)(2,1)}, u32[]{:S(2)}) copy-start(bf16[128,32]{0,1:T(8,128)(2,1)} %param.23) | copy-start | bytes 24580
  72.7 4.8 %copy-start.6 = (bf16[128,32]{0,1:T(8,128)(2,1)S(1)}, bf16[128,32]{0,1:T(8,128)(2,1)}, u32[]{:S(2)}) copy-start(bf16[128,32]{0,1:T(8,128)(2,1)} %param.22) | copy-start | bytes 24580
  72.7 5.6 %copy-start.8 = (bf16[3,128]{1,0:T(4,128)(2,1)S(1)}, bf16[3,128]{1,0:T(4,128)(2,1)}, u32[]{:S(2)}) copy-start(bf16[3,128]{1,0:T(4,128)(2,1)} %param.20) | copy-start | bytes 2308
  72.7 54.4 %all-to-all-start = ((bf16[8,2,131072]{2,1,0:T(2,128)(2,1)}), bf16[8,2,131072]{2,1,0:T(2,128)(2,1)}, u32[]{:S(2)}, u32[]{:S(2)}) async-start(bf16[8,2,131072]{2,1,0:T(2,128)(2,1)} %reshape.255), calls=%async_computation | async-start | bytes 8388608 | tf_op jit(solution)/shard_map/all_to_all | solution.py:14
  77.4 216.4 %all-gather.5.cloned.1.call-start = ((), (), s32[]{:S(2)}) async-start(), calls=%async_computation.3 | async-start | bytes 1064960 | tf_op jit(solution)/shard_map/all_gather | solution.py:35
  78.2 275.4 %reduce-scatter.2.cloned.1.call-start = ((), (), s32[]{:S(2)}) async-start(), calls=%async_computation.4 | async-start | bytes 4718592 | tf_op jit(solution)/shard_map/reduce_scatter | solution.py:141
  135.9 10.2 %copy-start.1 = (bf16[2048,1,1024]{2,1,0:T(2,128)(2,1)S(1)}, bf16[2048,1,1024]{2,1,0:T(2,128)(2,1)}, u32[]{:S(2)}) copy-start(bf16[2048,1,1024]{2,1,0:T(2,128)(2,1)} %reshape.256) | copy-start | bytes 12582916
  163.6 1.3 copy-start.4
  167.6 3.6 %copy-start = (bf16[1024,2048]{0,1:T(8,128)(2,1)S(1)}, bf16[1024,2048]{0,1:T(8,128)(2,1)}, u32[]{:S(2)}) copy-start(bf16[1024,2048]{0,1:T(8,128)(2,1)} %multiply_convert_fusion) | copy-start | bytes 12582916
  171.2 6.1 %copy-start.3 = (bf16[2048,640]{1,0:T(8,128)(2,1)S(1)}, bf16[2048,640]{1,0:T(8,128)(2,1)}, u32[]{:S(2)}) copy-start(bf16[2048,640]{1,0:T(8,128)(2,1)} %all-gather.3.cloned.1.call-done) | copy-start | bytes 7864324
  173.3 12.6 %collective-permute-start = (bf16[128,128]{0,1:T(8,128)(2,1)S(1)}, bf16[128,128]{0,1:T(8,128)(2,1)S(1)}, u32[]{:S(2)}, u32[]{:S(2)}) collective-permute-start(bf16[128,128]{0,1:T(8,128)(2,1)S(1)} %pad_maximum_fusion.3), channel_id=1, source_target_pairs={{0,32},{32,64},{64,96},{96,128},{128,160},{160,192},{192,224},{224... | collective-permute-start | bytes 98312 | tf_op jit(solution)/shard_map/ppermute | solution.py:29
  180.7 5.1 %collective-permute-start.1 = (bf16[2,128]{1,0:T(2,128)(2,1)S(1)}, bf16[2,128]{1,0:T(2,128)(2,1)S(1)}, u32[]{:S(2)}, u32[]{:S(2)}) collective-permute-start(bf16[2,128]{1,0:T(2,128)(2,1)S(1)} %slice.77), channel_id=1, source_target_pairs={{0,32},{32,64},{64,96},{96,128},{128,160},{160,192},{192,224},{224... | collective-permute-start | bytes 1544 | tf_op jit(solution)/shard_map/ppermute | solution.py:29
  185.5 1.3 copy-start.7
  293.9 5.7 %copy-start.2 = (bf16[2048,256]{1,0:T(8,128)(2,1)S(1)}, bf16[2048,256]{1,0:T(8,128)(2,1)}, u32[]{:S(2)}) copy-start(bf16[2048,256]{1,0:T(8,128)(2,1)} %all-gather.5.cloned.1.call-done) | copy-start | bytes 3145732
Sparse Core Ops, SparseCore 0:
  10.3 145.3 all-gather.2
  158.6 135.2 all-gather.4
  310.9 42.6 reduce-scatter.1
